TPU v7x, 256 devices: a whole 4x4x8 slice. The times are simulated.
256 devices in a mesh: sp: 32 (over z, x), fs: 4 (over y), tp: 2 (over core).
Axes of the slice: x: 4, y: 4, z: 8, core: 2. Of those that a mesh axis runs over, the one named last changes fastest.
Arguments:
- tokens: bfloat16 [4, 8192, 2048], P('fs', 'sp', 'tp'), may hold values from -6 to 6
- norm_gain: float32 [2048], replicated, may hold values from 0.1 to 1.9
- query_weight: bfloat16 [2048, 1024], P(('sp', 'fs'), 'tp'), may hold values from -0.125 to 0.125
- forget_weight: bfloat16 [2048, 1024], P(('sp', 'fs'), 'tp'), may hold values from -0.125 to 0.125
- value_weight: bfloat16 [2048, 1024], P(('sp', 'fs'), 'tp'), may hold values from -0.125 to 0.125
- outgate_weight: bfloat16 [2048, 1024], P(('sp', 'fs'), 'tp'), may hold values from -0.125 to 0.125
- pool_in_weight: bfloat16 [2048, 1024], P(('sp', 'fs'), 'tp'), may hold values from -0.125 to 0.125
- forget_room: float32 [1024], P('tp'), may hold values from 0 to 0.06
- decay_shift: float32 [4, 8192, 8], P('fs', 'sp', 'tp'), may hold values from -0.6 to 0
- head_gain: float32 [128], replicated, may hold values from 0.1 to 1.9
- start_state: float32 [4, 8, 128, 128], P('fs', 'tp'), may hold values from -0.03314563 to 0.03314563
- pool_map: bfloat16 [4, 256, 256], P('tp'), may hold values from -0.375 to 0.375
- pool_scale: float32 [1024], P('tp'), may hold values from 0.1 to 1.9
- out_rec_weight: bfloat16 [1024, 2048], P('tp', ('sp', 'fs')), may hold values from -0.125 to 0.125
- out_pool_weight: bfloat16 [1024, 2048], P('tp', ('sp', 'fs')), may hold values from -0.125 to 0.125
Outputs:
- mixed: bfloat16 [4, 8192, 2048], P('fs', ('sp', 'tp'))
All inputs are finite; a program needn't handle non-finite values.
Results may differ from a plain program's by a relative error of at most 0.013.
Values may be sent and summed in bfloat16 or wider, within the bound.
A program may use at most 128 MiB of HBM per device.

v0:
```python
import jax
import jax.numpy as jnp
from jax import lax
from jax.sharding import Mesh
from jax.sharding import PartitionSpec as P

HEAD = 128
POOL_DIM = 256
WIDEST = 16
BLOCK = 128
SP_FS = ("sp_0", "sp_1", "fs")
SP = ("sp_0", "sp_1")
SP_TP = ("sp_0", "sp_1", "tp")
EPSILON = 1e-06


def from_everyone(array, axis):
    count = lax.axis_size(axis)
    return lax.all_to_all(
        jnp.broadcast_to(array[None], (count, *array.shape)), axis, 0, 0, tiled=True
    )


def laid_out(blocks, dim):
    blocks = jnp.moveaxis(blocks, 0, dim)
    lengths = blocks.shape
    return blocks.reshape(*lengths[:dim], lengths[dim] * lengths[dim + 1], *lengths[dim + 2 :])


def gather_directly(array, axis, dim):
    blocks = from_everyone(array, axis)
    return laid_out(blocks, dim)


def gather_turned(arrays, axis, dims):
    turned = [jnp.moveaxis(a, dim, 0) for a, dim in zip(arrays, dims)]
    both = jnp.concatenate([t.reshape(len(t), -1) for t in turned], axis=1)
    filled, at, done = (lax.all_gather(both, axis, axis=0, tiled=True), 0, [])
    for t, dim in zip(turned, dims):
        slab = filled[:, at : at + t[0].size].reshape(-1, *t.shape[1:])
        done.append(jnp.moveaxis(slab, 0, dim))
        at += t[0].size
    return tuple(done)


def neutral_like(array, identity):
    return jax.tree.map(
        lambda part, zero: jnp.zeros_like(part) + jnp.asarray(zero, part.dtype), array, identity
    )


def entering_2(array, axes, combine, identity):
    before = start = neutral_like(array, identity)
    so_far = array
    for axis in reversed(axes):
        count, mine = (lax.axis_size(axis), lax.axis_index(axis))
        pieces = jax.tree.map(
            lambda part, kind: lax.all_gather(part.astype(kind), axis),
            so_far,
            (jnp.bfloat16, jnp.bfloat16),
        )
        inside, so_far = (start, start)
        for k in range(count):
            passed = k < mine
            so_far = combine(
                so_far, jax.tree.map(lambda part, own: part[k].astype(own.dtype), pieces, array)
            )
            inside = jax.tree.map(lambda new, old: jnp.where(passed, new, old), so_far, inside)
        before = combine(inside, before)
    return before


def shifted(value, axis, steps):
    count = lax.axis_size(axis)
    first, last = (max(0, -steps), min(count, count - steps))
    return lax.ppermute(value, axis, [(source, source + steps) for source in range(first, last)])


def in_blocks(array, dim, count):
    lengths = array.shape
    blocks = array.reshape(*lengths[:dim], count, lengths[dim] // count, *lengths[dim + 1 :])
    return jnp.moveaxis(blocks, dim, 0)


def sum_at_owner(array, axis, dim):
    blocks = in_blocks(array, dim, lax.axis_size(axis))
    arrived = lax.all_to_all(blocks, axis, split_axis=0, concat_axis=0, tiled=True)
    return arrived.astype(jnp.float32).sum(axis=0)


def rms_scale(entry_vectors):
    return lax.rsqrt(jnp.mean(entry_vectors * entry_vectors, axis=-1, keepdims=True) + EPSILON)


def compose(earlier, later):
    return (earlier[0] + later[0], jnp.exp(later[0])[:, :, None] * earlier[1] + later[1])


def per_device(
    tokens,
    norm_gain,
    query_weight,
    forget_weight,
    value_weight,
    outgate_weight,
    pool_in_weight,
    forget_room,
    decay_shift,
    head_gain,
    start_state,
    pool_map,
    pool_scale,
    out_rec_weight,
    out_pool_weight,
):
    widened = gather_directly(tokens, "tp", 2)[0].astype(jnp.float32)
    rescaled_input = (widened * rms_scale(widened) * norm_gain).astype(jnp.bfloat16)
    out_local = jnp.concatenate([out_rec_weight, out_pool_weight], axis=0)
    gathered = gather_turned(
        (query_weight, forget_weight, value_weight, outgate_weight, pool_in_weight, out_local),
        SP_FS,
        (0, 0, 0, 0, 0, 1),
    )
    projected = [
        jnp.dot(rescaled_input, weight, preferred_element_type=jnp.float32).astype(jnp.bfloat16)
        for weight in gathered[:5]
    ]
    length = rescaled_input.shape[0]
    head_count = forget_room.shape[0] // HEAD
    blocks = length // BLOCK
    queries = jax.nn.silu(projected[0].astype(jnp.float32)) * HEAD ** (-0.5)
    keyed = forget_room[None, :] * (1.0 - jax.nn.sigmoid(projected[1].astype(jnp.float32)))
    log_decay = jnp.log1p(-keyed).reshape(length, head_count, HEAD) + decay_shift[0][:, :, None]

    def to_blocks(entry_vectors):
        return entry_vectors.reshape(blocks, BLOCK, head_count, HEAD).transpose(2, 0, 1, 3)

    query_blocks = to_blocks(queries)
    key_blocks = to_blocks(keyed)
    value_blocks = to_blocks(projected[2])
    within = jnp.cumsum(to_blocks(log_decay), axis=2)
    centre = within[:, :, BLOCK // 2 - 1 : BLOCK // 2]
    ending = within[:, :, BLOCK - 1 : BLOCK]
    causal = jnp.tril(jnp.ones((BLOCK, BLOCK), jnp.float32))
    scores = (
        jnp.einsum(
            "hncd,hnsd->hncs",
            (query_blocks * jnp.exp(within - centre)).astype(jnp.bfloat16),
            (key_blocks * jnp.exp(centre - within)).astype(jnp.bfloat16),
            preferred_element_type=jnp.float32,
        )
        * causal
    )
    inside = jnp.einsum(
        "hncs,hnse->hnce",
        scores.astype(jnp.bfloat16),
        value_blocks,
        preferred_element_type=jnp.float32,
    )
    added = jnp.einsum(
        "hncd,hnce->nhde",
        (key_blocks * jnp.exp(ending - within)).astype(jnp.bfloat16),
        value_blocks,
        preferred_element_type=jnp.float32,
    )
    block_decay = ending[:, :, 0, :].transpose(1, 0, 2)

    def advance(memory, inputs):
        decay_piece, added_piece = inputs
        return (jnp.exp(decay_piece)[:, :, None] * memory + added_piece, memory)

    local_state, block_starts = lax.scan(
        advance, jnp.zeros((head_count, HEAD, HEAD), jnp.float32), (block_decay, added)
    )
    decay_before = jnp.cumsum(block_decay, axis=0) - block_decay
    local_decay = jnp.sum(block_decay, axis=0)
    identity = (jnp.zeros_like(local_decay), jnp.zeros_like(local_state))
    prefix_decay, prefix_state = entering_2((local_decay, local_state), SP, compose, identity)
    entering = prefix_state + jnp.exp(prefix_decay)[:, :, None] * start_state[0]
    block_states = block_starts + jnp.exp(decay_before)[:, :, :, None] * entering[None]
    carried = jnp.einsum(
        "hncd,nhde->hnce",
        (query_blocks * jnp.exp(within)).astype(jnp.bfloat16),
        block_states.astype(jnp.bfloat16),
        preferred_element_type=jnp.float32,
    )
    outputs = (inside + carried).transpose(1, 2, 0, 3).reshape(length, head_count, HEAD)
    gating = jax.nn.silu(projected[3].astype(jnp.float32)).reshape(length, head_count, HEAD)
    rec_out = (outputs * rms_scale(outputs) * head_gain * gating).reshape(length, head_count * HEAD)
    rec_out = rec_out.astype(jnp.bfloat16)
    pool_input = projected[4]
    columns = pool_input.shape[1]
    border = shifted(pool_input[length - WIDEST :], SP, 1)
    extended = jnp.concatenate([border, pool_input], axis=0).astype(jnp.float32)
    feature_lane = lax.axis_index("tp") * columns + jnp.arange(columns, dtype=jnp.int32)
    reach = jnp.left_shift(jnp.int32(2), feature_lane // POOL_DIM)
    window_sum = jnp.zeros((length, columns), jnp.float32)
    for offset in range(WIDEST):
        window_sum = window_sum + extended[WIDEST - offset : WIDEST - offset + length] * (
            offset < reach
        ).astype(jnp.float32)
    position = lax.axis_index(SP) * length + jnp.arange(length, dtype=jnp.int32)
    amount = jnp.minimum(position[:, None] + 1, reach[None, :]).astype(jnp.float32)
    pooled = (window_sum / amount - extended[WIDEST:]).astype(jnp.bfloat16)
    group_count = pool_map.shape[0]
    mapped = jnp.einsum(
        "tgc,gcd->tgd",
        pooled.reshape(length, group_count, POOL_DIM),
        pool_map,
        preferred_element_type=jnp.float32,
    )
    pool_out = (mapped.reshape(length, columns) * pool_scale).astype(jnp.bfloat16)
    joined = jnp.concatenate([rec_out, pool_out], axis=1)
    out_whole = gathered[5]
    mixed_rows = sum_at_owner(
        jnp.dot(joined, out_whole, preferred_element_type=jnp.float32).astype(jnp.bfloat16), "tp", 0
    )
    return mixed_rows.astype(jnp.bfloat16)[None]


def solution(mesh):
    finer = Mesh(
        mesh.devices.reshape(8, 4, mesh.shape["fs"], mesh.shape["tp"]), ("sp_0", "sp_1", "fs", "tp")
    )
    placed = (
        P("fs", SP, "tp"),
        P(),
        P(SP_FS, "tp"),
        P(SP_FS, "tp"),
        P(SP_FS, "tp"),
        P(SP_FS, "tp"),
        P(SP_FS, "tp"),
        P("tp"),
        P("fs", SP, "tp"),
        P(),
        P("fs", "tp", None, None),
        P("tp", None, None),
        P("tp"),
        P("tp", SP_FS),
        P("tp", SP_FS),
    )
    return jax.shard_map(
        per_device, mesh=finer, in_specs=placed, out_specs=P("fs", SP_TP, None), check_vma=False
    )
```

profile of v0, /device:TPU:1, one launch (start us, length us, event | category | flops | bytes accessed | tf_op | source)
XLA Modules:
  0.0 264.8 jit_solution(8559160675575011905)
XLA Ops:
  6.5 0.8 constant_dynamic-update-slice_fusion.4
  11.6 1.2 copy.43
  12.9 1.1 broadcast_in_dim.22
  13.9 6.8 %all-to-all-start = ((bf16[2,1,256,1024]{2,3,1,0:T(8,128)(2,1)}), bf16[2,1,256,1024]{2,3,1,0:T(8,128)(2,1)S(1)}, u32[]{:S(2)}, u32[]{:S(2)}) async-start(bf16[2,1,256,1024]{2,3,1,0:T(8,128)(2,1)} %broadcast_in_dim.22), calls=%async_computation | async-start | bytes 2097152 | tf_op jit(solution)/shard_map/all_to_all | solution.py:19
  26.4 131.7 %all-gather.6.cloned.1.call-done = bf16[2048,3584]{1,0:T(8,128)(2,1)} async-done(((bf16[16,3584]{1,0:T(8,128)(2,1)}), bf16[2048,3584]{1,0:T(8,128)(2,1)}) %all-gather.6.cloned.1.call-update) | async-done | bytes 14680080 | tf_op jit(solution)/shard_map/all_gather | solution.py:38
  158.1 2.5 negate_log-plus-one_fusion
  161.6 7.6 %all-gather.2 = bf16[4,4,128]{2,1,0:T(4,128)(2,1)S(1)} all-gather(bf16[1,4,128]{2,1,0:T(4,128)(2,1)S(1)} %bitcast.212), channel_id=2, replica_groups=mesh['sp_0'=8,'sp_1'=4,'fs'=4,'tp'=2] {'sp_1'}, dimensions={0}, use_global_device_ids=true | all-gather | bytes 5120 | tf_op jit(solution)/shard_map/all_gather | solution.py:58
  169.3 11.1 %all_gather.23 = bf16[8,4,128]{2,1,0:T(4,128)(2,1)S(1)} all-gather(bf16[1,4,128]{2,1,0:T(4,128)(2,1)S(1)} %get-tuple-element.93), channel_id=1, replica_groups=mesh['sp_0'=8,'sp_1'=4,'fs'=4,'tp'=2] {'sp_0'}, dimensions={0}, use_global_device_ids=true | all-gather | bytes 9216 | tf_op jit(solution)/shard_map/all_gather | solution.py:58
  180.6 2.3 fusion.24
  183.3 1.9 while.13
  185.2 9.9 %all-gather.1 = bf16[16,128,128]{2,1,0:T(8,128)(2,1)S(1)} all-gather(bf16[4,128,128]{2,1,0:T(8,128)(2,1)S(1)} %convert_element_type.456), channel_id=3, replica_groups=mesh['sp_0'=8,'sp_1'=4,'fs'=4,'tp'=2] {'sp_1'}, dimensions={0}, use_global_device_ids=true | all-gather | bytes 655360 | tf_op jit(solution)/shard_map/all_gather | solution.py:58
  195.7 1.0 fusion.118
  196.7 2.7 %multiply_multiply_fusion = f32[256,512]{1,0:T(8,128)S(1)} fusion(bf16[256,2048]{0,1:T(8,128)(2,1)} %copy-done.1, bf16[2048,3584]{1,0:T(8,128)(2,1)} %all-gather.6.cloned.1.call-done), kind=kOutput, calls=%fused_computation.94 | convolution fusion | flops 537788416 | bytes 3670016 | tf_op jit(solution)/shard_map/dot_general | solution.py:125
  199.6 2.6 fusion.30
  202.4 1.3 collective-permute-start
  203.7 1.3 fusion.61
  205.2 1.0 fusion.94
  206.9 29.0 %all-gather.8.cloned.1.call-done = bf16[8,4,128,128]{3,2,1,0:T(8,128)(2,1)} async-done(((bf16[1,4,128,128]{3,2,1,0:T(8,128)(2,1)}), bf16[8,4,128,128]{3,2,1,0:T(8,128)(2,1)}) %all-gather.8.cloned.1.call-update) | async-done | bytes 1048592 | tf_op jit(solution)/shard_map/all_gather | solution.py:58
  236.0 2.2 fusion.110
  238.2 1.7 multiply_reduce_fusion.1
  240.7 2.7 %fusion.64 = bf16[256,512]{1,0:T(8,128)(2,1)S(1)} fusion(f32[32,8,4,128]{3,2,1,0:T(4,128)S(1)} %bitcast.202, f32[32,8,4,128]{3,2,1,0:T(4,128)S(1)} %bitcast.205, bf16[256,2048]{0,1:T(8,128)(2,1)} %copy-done.1, bf16[2048,3584]{1,0:T(8,128)(2,1)} %all-gather.6.cloned.1.call-done, f32[512]{0:T(512)S(1)} %copy-done.19), kind=kOutput, calls=%fused_computation.44 | convolution fusion | flops 538181632 | bytes 4458496 | tf_op jit(solution)/shard_map/dot_general | solution.py:125
  243.4 3.5 %fusion.2 = bf16[256,2048]{1,0:T(8,128)(2,1)S(1)} fusion(bf16[2048,3584]{1,0:T(8,128)(2,1)} %all-gather.6.cloned.1.call-done, bf16[256,512]{1,0:T(8,128)(2,1)S(1)} %multiply_convert_fusion, bf16[256,512]{1,0:T(8,128)(2,1)S(1)} %fusion.64), kind=kOutput, calls=%fused_computation.6 | convolution fusion | flops 1075314688 | bytes 5767168 | tf_op jit(solution)/shard_map/dot_general | solution.py:216
  246.9 9.9 %all_to_all.10 = bf16[2,128,2048]{2,1,0:T(8,128)(2,1)S(1)} all-to-all(bf16[2,128,2048]{2,1,0:T(8,128)(2,1)S(1)} %bitcast.200), channel_id=1, replica_groups=mesh['sp_0'=8,'sp_1'=4,'fs'=4,'tp'=2] {'tp'}, dimensions={0} | all-to-all | bytes 2097152 | tf_op jit(solution)/shard_map/all_to_all | solution.py:87
  256.8 1.1 reduce_sum.42
  (109 shorter events, 15.6 us)
Async XLA Ops:
  6.5 199.7 %copy-start = (bf16[2,256,256]{2,1,0:T(8,128)(2,1)S(1)}, bf16[2,256,256]{2,1,0:T(8,128)(2,1)}, u32[]{:S(2)}) copy-start(bf16[2,256,256]{2,1,0:T(8,128)(2,1)} %param.28) | copy-start | bytes 786436
  6.5 151.6 %all-gather.6.cloned.1.call-start = ((), (), s32[]{:S(2)}) async-start(), calls=%async_computation.2 | async-start | bytes 14794752 | tf_op jit(solution)/shard_map/all_gather | solution.py:38
  12.8 7.9 %copy-start.17 = (f32[1,256,4]{1,2,0:T(4,128)S(1)}, f32[1,256,4]{1,2,0:T(4,128)}, u32[]{:S(2)}) copy-start(f32[1,256,4]{1,2,0:T(4,128)} %param.25) | copy-start | bytes 12292
  12.8 12.5 %copy-start.21 = (f32[128]{0:T(128)S(1)}, f32[128]{0:T(128)}, u32[]{:S(2)}) copy-start(f32[128]{0:T(128)} %param.26) | copy-start | bytes 1540
  13.9 11.1 %all-to-all-start = ((bf16[2,1,256,1024]{2,3,1,0:T(8,128)(2,1)}), bf16[2,1,256,1024]{2,3,1,0:T(8,128)(2,1)S(1)}, u32[]{:S(2)}, u32[]{:S(2)}) async-start(bf16[2,1,256,1024]{2,3,1,0:T(8,128)(2,1)} %broadcast_in_dim.22), calls=%async_computation | async-start | bytes 2097152 | tf_op jit(solution)/shard_map/all_to_all | solution.py:19
  20.7 215.2 %all-gather.8.cloned.1.call-start = ((), (), s32[]{:S(2)}) async-start(), calls=%async_computation.3 | async-start | bytes 1179648 | tf_op jit(solution)/shard_map/all_gather | solution.py:58
  26.1 132.0 %copy-start.22 = (f32[512]{0:T(512)S(1)}, f32[512]{0:T(512)}, u32[]{:S(2)}) copy-start(f32[512]{0:T(512)} %param.24) | copy-start | bytes 6148
  26.4 154.1 %copy-start.1 = (bf16[256,2048]{0,1:T(8,128)(2,1)}, bf16[256,2048]{0,1:T(8,128)(2,1)S(1)}, u32[]{:S(2)}) copy-start(bf16[256,2048]{0,1:T(8,128)(2,1)S(1)} %fusion.16) | copy-start | bytes 3145732
  202.3 2.8 %copy-start.5 = (f32[512]{0:T(512)S(1)}, f32[512]{0:T(512)}, u32[]{:S(2)}) copy-start(f32[512]{0:T(512)} %get-tuple-element.107) | copy-start | bytes 6148
  202.3 2.8 %copy-start.6 = (f32[512]{0:T(512)S(1)}, f32[512]{0:T(512)}, u32[]{:S(2)}) copy-start(f32[512]{0:T(512)} %get-tuple-element.108) | copy-start | bytes 6148
  202.3 2.8 %copy-start.7 = (f32[512]{0:T(512)S(1)}, f32[512]{0:T(512)}, u32[]{:S(2)}) copy-start(f32[512]{0:T(512)} %get-tuple-element.109) | copy-start | bytes 6148
  202.3 2.8 %copy-start.8 = (f32[512]{0:T(512)S(1)}, f32[512]{0:T(512)}, u32[]{:S(2)}) copy-start(f32[512]{0:T(512)} %get-tuple-element.110) | copy-start | bytes 6148
  202.3 2.8 %copy-start.9 = (f32[512]{0:T(512)S(1)}, f32[512]{0:T(512)}, u32[]{:S(2)}) copy-start(f32[512]{0:T(512)} %get-tuple-element.111) | copy-start | bytes 6148
  202.3 2.8 %copy-start.10 = (f32[512]{0:T(512)S(1)}, f32[512]{0:T(512)}, u32[]{:S(2)}) copy-start(f32[512]{0:T(512)} %get-tuple-element.112) | copy-start | bytes 6148
  202.3 2.8 %copy-start.11 = (f32[512]{0:T(512)S(1)}, f32[512]{0:T(512)}, u32[]{:S(2)}) copy-start(f32[512]{0:T(512)} %get-tuple-element.113) | copy-start | bytes 6148
  202.3 2.8 %copy-start.12 = (f32[512]{0:T(512)S(1)}, f32[512]{0:T(512)}, u32[]{:S(2)}) copy-start(f32[512]{0:T(512)} %get-tuple-element.114) | copy-start | bytes 6148
  202.3 2.8 %copy-start.13 = (f32[512]{0:T(512)S(1)}, f32[512]{0:T(512)}, u32[]{:S(2)}) copy-start(f32[512]{0:T(512)} %get-tuple-element.115) | copy-start | bytes 6148
  202.4 2.8 %copy-start.14 = (f32[512]{0:T(512)S(1)}, f32[512]{0:T(512)}, u32[]{:S(2)}) copy-start(f32[512]{0:T(512)} %get-tuple-element.116) | copy-start | bytes 6148
  202.4 2.8 %copy-start.15 = (f32[512]{0:T(512)S(1)}, f32[512]{0:T(512)}, u32[]{:S(2)}) copy-start(f32[512]{0:T(512)} %get-tuple-element.117) | copy-start | bytes 6148
  202.4 2.8 %copy-start.20 = (s32[256]{0:T(256)S(1)}, s32[256]{0:T(256)}, u32[]{:S(2)}) copy-start(s32[256]{0:T(256)} %add_add_fusion) | copy-start | bytes 3076
  202.4 2.6 collective-permute-start
  206.2 29.7 %copy-start.2 = (f32[1,4,128,128]{3,2,1,0:T(8,128)S(1)}, f32[1,4,128,128]{3,2,1,0:T(8,128)}, u32[]{:S(2)}) copy-start(f32[1,4,128,128]{3,2,1,0:T(8,128)} %param.27) | copy-start | bytes 786436
  206.2 29.7 %copy-start.16 = (f32[4,128]{1,0:T(4,128)S(1)}, f32[4,128]{1,0:T(4,128)}, u32[]{:S(2)}) copy-start(f32[4,128]{1,0:T(4,128)} %get-tuple-element.78) | copy-start | bytes 6148
  238.2 2.5 copy-start.19
  (3 other events, 2.4 us)
Sparse Core Ops, SparseCore 0:
  11.7 146.3 all-gather.5
  196.8 39.0 all-gather.7
where the time goes:
time: 266 us; the launch traced here: 265 us
  waiting for transfers between devices  161 us (61%)
  blocking collectives  38.6 us (15%)
  matrix products  20 us (8%)
  other arithmetic  14.4 us (5%)
  between operations  14 us (5%)
  local copies, waits for them, and re-layouts  9.02 us (3%)
  starting transfers between devices  8.06 us (3%)
    all_gather x1, waiting for transfers between devices, gather_turned(): filled, at, done = (lax.all_gather(both, axis, axis=0, tiled=True), 0, [])  132 us
    all_gather x1, waiting for transfers between devices, entering_2(): lax.all_gather(part.astype(kind), axis)  29 us
    all_gather x3, blocking collectives, entering_2(): lax.all_gather(part.astype(kind), axis)  28.7 us
    dot_general x5, matrix products, per_device(): jnp.dot(rescaled_input, weight, preferred_element_type=jnp.float32)  12.9 us
    all_to_all x1, blocking collectives, sum_at_owner(): lax.all_to_all(blocks, axis, split_axis=0, concat_axis=0, tiled=True)  9.93 us
    all_to_all x1, starting transfers between devices, from_everyone(): lax.all_to_all(jnp.broadcast_to(array[None], (count, *array.shape)), axis...  6.77 us
  transfers between devices with their start and end apart: 4, of which 2 were waited for; matrix products, arithmetic and copies ran while one was open for 6% of the time, Pallas kernels for 0%

commit v1 on v0

--- a/solution.py
+++ b/solution.py
@@ -35,7 +35,13 @@
 def gather_turned(arrays, axis, dims):
     turned = [jnp.moveaxis(a, dim, 0) for a, dim in zip(arrays, dims)]
     both = jnp.concatenate([t.reshape(len(t), -1) for t in turned], axis=1)
-    filled, at, done = (lax.all_gather(both, axis, axis=0, tiled=True), 0, [])
+    filled, at, done = (
+        jnp.concatenate(
+            lax.all_to_all(jnp.stack([both] * lax.axis_size(axis)), axis, 0, 0), axis=0
+        ),
+        0,
+        [],
+    )
     for t, dim in zip(turned, dims):
         slab = filled[:, at : at + t[0].size].reshape(-1, *t.shape[1:])
         done.append(jnp.moveaxis(slab, 0, dim))

time: 266 us -> 467 us (1.76)
  waiting for transfers between devices: 161 us -> 340 us
  starting transfers between devices: 8.06 us -> 22.5 us
    all_to_all x0 -> x1, waiting for transfers between devices: none -> 320 us  [gather_turned(): lax.all_to_all(jnp.stack([both] * lax.axis_size(axis)), axis, 0, 0)]
    all_gather x1 -> x0, waiting for transfers between devices: 132 us -> none  [gather_turned(): filled, at, done = (lax.all_gather(both, axis, axis=0, tiled=True), 0, [])]
    all_to_all x0 -> x1, starting transfers between devices: none -> 14.4 us  [gather_turned(): lax.all_to_all(jnp.stack([both] * lax.axis_size(axis)), axis, 0, 0)]
    all_gather x1, waiting for transfers between devices: 29 us -> 18 us  [entering_2(): lax.all_gather(part.astype(kind), axis)]
    another operation x0 -> x1, local copies, waits for them, and re-layouts: none -> 6.98 us  [gather_turned(): jnp.stack([both] * lax.axis_size(axis))]
  transfers between devices with their start and end apart: 4 -> 4, of which waited for: 2 -> 3; matrix products, arithmetic and copies ran while one was open for 6% -> 4% of each run, Pallas kernels for 0% -> 0%
where the time goes in v1:
time: 467 us; the launch traced here: 466 us
  waiting for transfers between devices  340 us (73%)
  blocking collectives  42.6 us (9%)
  starting transfers between devices  22.5 us (5%)
  other arithmetic  17.9 us (4%)
  matrix products  17.2 us (4%)
  between operations  14 us (3%)
  local copies, waits for them, and re-layouts  11.8 us (3%)
    all_to_all x1, waiting for transfers between devices, gather_turned(): lax.all_to_all(jnp.stack([both] * lax.axis_size(axis)), axis, 0, 0)  320 us
    all_gather x3, blocking collectives, entering_2(): lax.all_gather(part.astype(kind), axis)  32.8 us
    all_gather x1, waiting for transfers between devices, entering_2(): lax.all_gather(part.astype(kind), axis)  18 us
    all_to_all x1, starting transfers between devices, gather_turned(): lax.all_to_all(jnp.stack([both] * lax.axis_size(axis)), axis, 0, 0)  14.4 us
    dot_general x5, matrix products, per_device(): jnp.dot(rescaled_input, weight, preferred_element_type=jnp.float32)  12.1 us
    all_to_all x1, blocking collectives, sum_at_owner(): lax.all_to_all(blocks, axis, split_axis=0, concat_axis=0, tiled=True)  9.9 us
  transfers between devices with their start and end apart: 4, of which 3 were waited for; matrix products, arithmetic and copies ran while one was open for 4% of the time, Pallas kernels for 0%

profile of v1, /device:TPU:1, one launch (start us, length us, event | category | flops | bytes accessed | tf_op | source)
XLA Modules:
  0.0 466.1 jit_solution(18025769354872571228)
XLA Ops:
  6.5 1.3 copy.43
  7.9 1.1 broadcast_in_dim.22
  9.0 6.8 %all-to-all-start = ((bf16[2,1,256,1024]{2,3,1,0:T(8,128)(2,1)}), bf16[2,1,256,1024]{2,3,1,0:T(8,128)(2,1)S(1)}, u32[]{:S(2)}, u32[]{:S(2)}) async-start(bf16[2,1,256,1024]{2,3,1,0:T(8,128)(2,1)} %broadcast_in_dim.22), calls=%async_computation | async-start | bytes 2097152 | tf_op jit(solution)/shard_map/all_to_all | solution.py:19
  15.9 1.6 all-to-all-done
  17.5 7.0 %stack.2 = bf16[128,16,3584]{2,1,0:T(8,128)(2,1)} broadcast(bf16[16,3584]{1,0:T(8,128)(2,1)S(1)} %fusion.123), dimensions={1,2} | broadcast | bytes 14794752 | tf_op jit(solution)/shard_map/stack | solution.py:40
  24.5 14.4 %all-to-all-start.1 = ((bf16[128,16,3584]{2,1,0:T(8,128)(2,1)}), bf16[128,16,3584]{2,1,0:T(8,128)(2,1)}, u32[]{:S(2)}, u32[]{:S(2)}) async-start(bf16[128,16,3584]{2,1,0:T(8,128)(2,1)} %stack.2), calls=%async_computation.1 | async-start | bytes 29360128 | tf_op jit(solution)/shard_map/all_to_all | solution.py:40
  46.4 320.3 %all-to-all-done.1 = bf16[128,16,3584]{2,1,0:T(8,128)(2,1)} async-done(((bf16[128,16,3584]{2,1,0:T(8,128)(2,1)}), bf16[128,16,3584]{2,1,0:T(8,128)(2,1)}, u32[]{:S(2)}, u32[]{:S(2)}) %all-to-all-start.1) | async-done | bytes 14680096 | tf_op jit(solution)/shard_map/all_to_all | solution.py:40
  366.7 2.3 fusion.30
  369.1 2.5 multiply_multiply_fusion
  371.6 2.3 fusion.24
  373.9 1.3 collective-permute-start
  375.2 2.5 negate_log-plus-one_fusion
  379.5 1.9 while.13
  381.4 7.5 %all-gather.2 = bf16[4,4,128]{2,1,0:T(4,128)(2,1)S(1)} all-gather(bf16[1,4,128]{2,1,0:T(4,128)(2,1)S(1)} %bitcast.212), channel_id=2, replica_groups=mesh['sp_0'=8,'sp_1'=4,'fs'=4,'tp'=2] {'sp_1'}, dimensions={0}, use_global_device_ids=true | all-gather | bytes 5120 | tf_op jit(solution)/shard_map/all_gather | solution.py:64
  388.9 10.4 %all-gather.1 = bf16[16,128,128]{2,1,0:T(8,128)(2,1)S(1)} all-gather(bf16[4,128,128]{2,1,0:T(8,128)(2,1)S(1)} %convert_element_type.456), channel_id=3, replica_groups=mesh['sp_0'=8,'sp_1'=4,'fs'=4,'tp'=2] {'sp_1'}, dimensions={0}, use_global_device_ids=true | all-gather | bytes 655360 | tf_op jit(solution)/shard_map/all_gather | solution.py:64
  401.0 14.8 %all_gather.19 = bf16[8,4,128]{2,1,0:T(4,128)(2,1)S(1)} all-gather(bf16[1,4,128]{2,1,0:T(4,128)(2,1)S(1)} %get-tuple-element.93), channel_id=1, replica_groups=mesh['sp_0'=8,'sp_1'=4,'fs'=4,'tp'=2] {'sp_0'}, dimensions={0}, use_global_device_ids=true | all-gather | bytes 9216 | tf_op jit(solution)/shard_map/all_gather | solution.py:64
  416.3 1.0 maximum_convert_fusion
  417.3 1.8 fusion.94
  420.5 18.0 %all-gather.5.cloned.1.call-done = bf16[8,4,128,128]{3,2,1,0:T(8,128)(2,1)} async-done(((bf16[1,4,128,128]{3,2,1,0:T(8,128)(2,1)}), bf16[8,4,128,128]{3,2,1,0:T(8,128)(2,1)}) %all-gather.5.cloned.1.call-update) | async-done | bytes 1048592 | tf_op jit(solution)/shard_map/all_gather | solution.py:64
  438.6 2.4 fusion.110
  442.3 2.4 fusion.64
  444.7 3.5 fusion.2
  448.2 9.9 %all_to_all.15 = bf16[2,128,2048]{2,1,0:T(8,128)(2,1)S(1)} all-to-all(bf16[2,128,2048]{2,1,0:T(8,128)(2,1)S(1)} %bitcast.201), channel_id=1, replica_groups=mesh['sp_0'=8,'sp_1'=4,'fs'=4,'tp'=2] {'tp'}, dimensions={0} | all-to-all | bytes 2097152 | tf_op jit(solution)/shard_map/all_to_all | solution.py:93
  458.1 1.1 reduce_sum.42
  (103 shorter events, 15.8 us)
Async XLA Ops:
  6.5 412.6 %copy-start = (bf16[2,256,256]{2,1,0:T(8,128)(2,1)S(1)}, bf16[2,256,256]{2,1,0:T(8,128)(2,1)}, u32[]{:S(2)}) copy-start(bf16[2,256,256]{2,1,0:T(8,128)(2,1)} %param.28) | copy-start | bytes 786436
  6.5 9.2 %copy-start.6 = (bf16[16,512]{1,0:T(8,128)(2,1)S(1)}, bf16[16,512]{1,0:T(8,128)(2,1)}, u32[]{:S(2)}) copy-start(bf16[16,512]{1,0:T(8,128)(2,1)} %param.19) | copy-start | bytes 49156
  7.8 7.9 %copy-start.7 = (bf16[16,512]{1,0:T(8,128)(2,1)S(1)}, bf16[16,512]{1,0:T(8,128)(2,1)}, u32[]{:S(2)}) copy-start(bf16[16,512]{1,0:T(8,128)(2,1)} %param.20) | copy-start | bytes 49156
  7.9 7.9 %copy-start.8 = (bf16[16,512]{1,0:T(8,128)(2,1)S(1)}, bf16[16,512]{1,0:T(8,128)(2,1)}, u32[]{:S(2)}) copy-start(bf16[16,512]{1,0:T(8,128)(2,1)} %param.21) | copy-start | bytes 49156
  7.9 7.9 %copy-start.9 = (bf16[16,512]{1,0:T(8,128)(2,1)S(1)}, bf16[16,512]{1,0:T(8,128)(2,1)}, u32[]{:S(2)}) copy-start(bf16[16,512]{1,0:T(8,128)(2,1)} %param.22) | copy-start | bytes 49156
  7.9 7.9 %copy-start.10 = (bf16[16,512]{1,0:T(8,128)(2,1)S(1)}, bf16[16,512]{1,0:T(8,128)(2,1)}, u32[]{:S(2)}) copy-start(bf16[16,512]{1,0:T(8,128)(2,1)} %param.23) | copy-start | bytes 49156
  7.9 8.0 %copy-start.11 = (bf16[512,16]{0,1:T(8,128)(2,1)S(1)}, bf16[512,16]{0,1:T(8,128)(2,1)}, u32[]{:S(2)}) copy-start(bf16[512,16]{0,1:T(8,128)(2,1)} %param.31) | copy-start | bytes 49156
  7.9 8.0 %copy-start.12 = (bf16[512,16]{0,1:T(8,128)(2,1)S(1)}, bf16[512,16]{0,1:T(8,128)(2,1)}, u32[]{:S(2)}) copy-start(bf16[512,16]{0,1:T(8,128)(2,1)} %param.30) | copy-start | bytes 49156
  9.0 8.5 %all-to-all-start = ((bf16[2,1,256,1024]{2,3,1,0:T(8,128)(2,1)}), bf16[2,1,256,1024]{2,3,1,0:T(8,128)(2,1)S(1)}, u32[]{:S(2)}, u32[]{:S(2)}) async-start(bf16[2,1,256,1024]{2,3,1,0:T(8,128)(2,1)} %broadcast_in_dim.22), calls=%async_computation | async-start | bytes 2097152 | tf_op jit(solution)/shard_map/all_to_all | solution.py:19
  24.5 14.5 %copy-start.15 = (f32[1,256,4]{1,2,0:T(4,128)S(1)}, f32[1,256,4]{1,2,0:T(4,128)}, u32[]{:S(2)}) copy-start(f32[1,256,4]{1,2,0:T(4,128)} %param.25) | copy-start | bytes 12292
  24.5 20.8 %copy-start.18 = (f32[128]{0:T(128)S(1)}, f32[128]{0:T(128)}, u32[]{:S(2)}) copy-start(f32[128]{0:T(128)} %param.26) | copy-start | bytes 1540
  24.5 342.2 %all-to-all-start.1 = ((bf16[128,16,3584]{2,1,0:T(8,128)(2,1)}), bf16[128,16,3584]{2,1,0:T(8,128)(2,1)}, u32[]{:S(2)}, u32[]{:S(2)}) async-start(bf16[128,16,3584]{2,1,0:T(8,128)(2,1)} %stack.2), calls=%async_computation.1 | async-start | bytes 29360128 | tf_op jit(solution)/shard_map/all_to_all | solution.py:40
  38.9 399.6 %all-gather.5.cloned.1.call-start = ((), (), s32[]{:S(2)}) async-start(), calls=%async_computation.3 | async-start | bytes 1179648 | tf_op jit(solution)/shard_map/all_gather | solution.py:64
  44.9 1.1 copy-start.13
  46.4 328.8 %copy-start.1 = (bf16[256,2048]{0,1:T(8,128)(2,1)}, bf16[256,2048]{0,1:T(8,128)(2,1)S(1)}, u32[]{:S(2)}) copy-start(bf16[256,2048]{0,1:T(8,128)(2,1)S(1)} %fusion.16) | copy-start | bytes 3145732
  369.0 4.8 %copy-start.4 = (bf16[256,512]{1,0:T(8,128)(2,1)}, bf16[256,512]{1,0:T(8,128)(2,1)S(1)}, u32[]{:S(2)}) copy-start(bf16[256,512]{1,0:T(8,128)(2,1)S(1)} %fusion.30) | copy-start | bytes 786436
  371.5 3.7 copy-start.19
  373.9 42.4 %collective-permute-start = (bf16[16,512]{1,0:T(8,128)(2,1)S(1)}, bf16[16,512]{1,0:T(8,128)(2,1)S(1)}, u32[]{:S(2)}, u32[]{:S(2)}) collective-permute-start(bf16[16,512]{1,0:T(8,128)(2,1)S(1)} %slice.240), channel_id=1, source_target_pairs={{0,8},{8,16},{16,24},{24,32},{32,40},{40,48},{48,56},{56,64},{64,7... | collective-permute-start | bytes 49160 | tf_op jit(solution)/shard_map/ppermute | solution.py:82
  419.1 0.7 copy-start.16
  419.1 19.5 %copy-start.14 = (f32[4,128]{1,0:T(4,128)S(1)}, f32[4,128]{1,0:T(4,128)}, u32[]{:S(2)}) copy-start(f32[4,128]{1,0:T(4,128)} %get-tuple-element.78) | copy-start | bytes 6148
  438.5 2.4 copy-start.3
  440.9 1.3 copy-start.2
  440.9 1.3 copy-start.17
  442.2 2.5 copy-start.5
Sparse Core Ops, SparseCore 0:
  401.1 37.3 all-gather.4
